TPU v7x, 32 devices: a whole 2x2x4 slice. The times are simulated.
32 devices in a mesh: grp: 2 (over y), sp: 4 (over z), tp: 4 (over x, core).
Axes of the slice: x: 2, y: 2, z: 4, core: 2. Of those that a mesh axis runs over, the one named last changes fastest.
Arguments:
- query_nope: bfloat16 [2560, 1024], P(('grp', 'sp'), 'tp'), parts along dimension 0, may hold values from -12 to 12
- query_rope: bfloat16 [2560, 512], P(('grp', 'sp'), 'tp'), parts along dimension 0, may hold values from -48 to 48
- token_latent: bfloat16 [2560, 256], P(('grp', 'sp')), parts along dimension 0, may hold values from -6 to 6
- key_rope: bfloat16 [2560, 32], P(('grp', 'sp')), parts along dimension 0, may hold values from -48 to 48
- latent_norm_gain: float32 [256], replicated, may hold values from 0.1 to 1.9
- key_expand_weight: bfloat16 [256, 1024], replicated, may hold values from -0.375 to 0.375
- value_expand_weight: bfloat16 [256, 1024], replicated, may hold values from -0.375 to 0.375
- residual: bfloat16 [2560, 2048], P(('grp', 'sp')), parts along dimension 0, may hold values from -3 to 3
- out_weight: bfloat16 [1024, 2048], P('tp'), may hold values from -0.375 to 0.375
- ffn_gain: float32 [2048], replicated, may hold values from 0.1 to 1.9
- gate_weight: bfloat16 [2048, 5632], P('sp', 'tp'), may hold values from -0.125 to 0.125
- up_weight: bfloat16 [2048, 5632], P('sp', 'tp'), may hold values from -0.125 to 0.125
- down_weight: bfloat16 [5632, 2048], P('tp', 'sp'), may hold values from -0.078125 to 0.078125
Outputs:
- layer_output: bfloat16 [2560, 2048], P(('grp', 'sp', 'tp')), parts along dimension 0
There are 2 independent parts, one for each index of `grp`. A program takes and returns all parts, laid end to end along the dimension named above; an argument that names none is the same for every part. Nothing has to cross between parts.
All inputs are finite; a program needn't handle non-finite values.
Results may differ from a plain program's by a relative error of at most 0.015.
Values may be sent and summed in bfloat16 or wider, within the bound.
A program may use at most 128 MiB of HBM per device.

v0:
```python
import jax
import jax.numpy as jnp
from jax import lax
from jax.sharding import PartitionSpec as P

UNROTATED_SIZE = 64
ROPE = 32
VALUE_SIZE = 64
GRID_W = 64


def norm_rows(values, gain):
    wide = values.astype(jnp.float32)
    return wide * lax.rsqrt(jnp.mean(wide * wide, axis=-1, keepdims=True) + 1e-06) * gain


def turn_heads(vectors, positions):
    tokens, heads, width = vectors.shape
    freqs = width // 4
    grid_pos = jnp.stack([positions // GRID_W, positions % GRID_W], axis=-1).astype(jnp.float32)
    inverse = jnp.power(10000.0, -jnp.arange(freqs, dtype=jnp.float32) / freqs)
    angles = grid_pos[:, :, None] * inverse
    cosine = jnp.cos(angles)[:, None]
    sine = jnp.sin(angles)[:, None]
    viewed = vectors.reshape(tokens, heads, 2, 2, freqs)
    first = viewed[..., 0, :]
    second = viewed[..., 1, :]
    turned = jnp.stack([first * cosine - second * sine, first * sine + second * cosine], axis=-2)
    return turned.reshape(tokens, heads, width)


def local(
    query_nope,
    query_rope,
    token_latent,
    key_rope,
    latent_norm_gain,
    key_expand_weight,
    value_expand_weight,
    residual,
    out_weight,
    ffn_gain,
    gate_weight,
    up_weight,
    down_weight,
):
    tok_rows = query_nope.shape[0]
    heads_here = query_nope.shape[1] // UNROTATED_SIZE
    own_rows = tok_rows // lax.axis_size("tp")
    tp_index = lax.axis_index("tp")
    positions = lax.axis_index("sp") * tok_rows + jnp.arange(tok_rows, dtype=jnp.int32)
    query_flat = query_nope.reshape(tok_rows, heads_here, UNROTATED_SIZE)
    query_turned = turn_heads(
        query_rope.astype(jnp.float32).reshape(tok_rows, heads_here, ROPE), positions
    ).astype(jnp.bfloat16)
    latent = norm_rows(token_latent, latent_norm_gain).astype(jnp.bfloat16)
    key_turned = turn_heads(key_rope.astype(jnp.float32)[:, None, :], positions)[:, 0].astype(
        jnp.bfloat16
    )
    key_cols = lax.dynamic_slice_in_dim(
        key_expand_weight, tp_index * heads_here * UNROTATED_SIZE, heads_here * UNROTATED_SIZE, 1
    )
    value_cols = lax.dynamic_slice_in_dim(
        value_expand_weight, tp_index * heads_here * VALUE_SIZE, heads_here * VALUE_SIZE, 1
    )
    score_scale = (UNROTATED_SIZE + ROPE) ** (-0.5)

    def absorb(carried, block_in):
        latent_block, rope_block = block_in
        block_rows = latent_block.shape[0]
        key_rows = jnp.dot(latent_block, key_cols, preferred_element_type=jnp.float32).astype(
            jnp.bfloat16
        )
        key_rows = key_rows.reshape(block_rows, heads_here, UNROTATED_SIZE)
        value_rows = jnp.dot(latent_block, value_cols, preferred_element_type=jnp.float32).astype(
            jnp.bfloat16
        )
        value_rows = value_rows.reshape(block_rows, heads_here, VALUE_SIZE)
        scores = (
            jnp.einsum("qhd,khd->hqk", query_flat, key_rows, preferred_element_type=jnp.float32)
            + jnp.einsum(
                "qhd,kd->hqk", query_turned, rope_block, preferred_element_type=jnp.float32
            )
        ) * score_scale
        highest, totals, accumulated = carried
        new_highest = jnp.maximum(highest, jnp.max(scores, axis=-1))
        shrink = jnp.exp(highest - new_highest)
        weights = jnp.exp(scores - new_highest[:, :, None])
        totals = totals * shrink + jnp.sum(weights, axis=-1)
        accumulated = accumulated * shrink.T[:, :, None] + jnp.einsum(
            "hqk,khd->qhd",
            weights.astype(jnp.bfloat16),
            value_rows,
            preferred_element_type=jnp.float32,
        )
        return ((new_highest, totals, accumulated), None)

    initial = (
        jnp.full((heads_here, tok_rows), -jnp.inf, jnp.float32),
        jnp.zeros((heads_here, tok_rows), jnp.float32),
        jnp.zeros((tok_rows, heads_here, VALUE_SIZE), jnp.float32),
    )
    carried = initial
    latent_piece = lax.all_gather(latent, "sp", axis=0, tiled=True)
    rope_piece = lax.all_gather(key_turned, "sp", axis=0, tiled=True)
    shard_count = latent_piece.shape[0] // tok_rows
    grouped = max(
        (
            factor
            for factor in range(1, shard_count + 1)
            if shard_count % factor == 0 and factor * tok_rows <= max(1024, tok_rows)
        )
    )
    block_rows = grouped * tok_rows
    blocks = (
        latent_piece.reshape(-1, block_rows, latent_piece.shape[1]),
        rope_piece.reshape(-1, block_rows, rope_piece.shape[1]),
    )
    carried, _ = lax.scan(absorb, carried, blocks)
    highest, totals, accumulated = carried
    attended = (
        (accumulated / totals.T[:, :, None])
        .reshape(tok_rows, heads_here * VALUE_SIZE)
        .astype(jnp.bfloat16)
    )
    projected = jnp.dot(attended, out_weight, preferred_element_type=jnp.float32).astype(
        jnp.bfloat16
    )
    summed = lax.psum(projected, "tp").astype(jnp.float32)
    mixed_all = residual.astype(jnp.float32) + summed
    normed_all = norm_rows(mixed_all, ffn_gain).astype(jnp.bfloat16)
    mixed_own = lax.dynamic_slice_in_dim(mixed_all, tp_index * own_rows, own_rows, 0)
    gate_piece = lax.all_gather(gate_weight, "sp", axis=0, tiled=True)
    up_piece = lax.all_gather(up_weight, "sp", axis=0, tiled=True)
    gate = jnp.dot(normed_all, gate_piece, preferred_element_type=jnp.float32)
    up_part = jnp.dot(normed_all, up_piece, preferred_element_type=jnp.float32)
    hidden = (jax.nn.silu(gate) * up_part).astype(jnp.bfloat16)
    terms = jnp.dot(
        hidden,
        lax.all_gather(down_weight, "sp", axis=1, tiled=True),
        preferred_element_type=jnp.float32,
    )
    ffn_own = lax.psum_scatter(
        terms.astype(jnp.bfloat16), "tp", scatter_dimension=0, tiled=True
    ).astype(jnp.float32)
    return (mixed_own + ffn_own).astype(jnp.bfloat16)


def solution(mesh):
    return jax.shard_map(
        local,
        mesh=mesh,
        in_specs=(
            P(("grp", "sp"), "tp"),
            P(("grp", "sp"), "tp"),
            P(("grp", "sp"), None),
            P(("grp", "sp"), None),
            P(),
            P(),
            P(),
            P(("grp", "sp"), None),
            P("tp", None),
            P(),
            P("sp", "tp"),
            P("sp", "tp"),
            P("tp", "sp"),
        ),
        out_specs=P(("grp", "sp", "tp"), None),
        check_vma=False,
    )
```

profile of v0, /device:TPU:0, one launch (start us, length us, event | category | flops | bytes accessed | tf_op | source)
XLA Modules:
  0.0 428.1 jit_solution(11533256106749414533)
XLA Ops:
  7.4 0.0 copy-start
  7.4 0.0 all-reduce.2.cloned.1.call-start
  7.4 1.1 copy.26
  8.6 0.7 convert.18
  9.3 0.2 multiply_cosine_fusion
  9.5 0.2 fusion.32
  9.7 15.1 %all-gather = bf16[4,320,32]{1,2,0:T(8,128)(2,1)S(1)} all-gather(bf16[1,320,32]{1,2,0:T(8,128)(2,1)S(1)} %bitcast.82), channel_id=1, replica_groups=mesh['grp'=2,'sp'=4,'tp'=4] {'sp'}, dimensions={0}, use_global_device_ids=true | all-gather | bytes 102400 | tf_op jit(solution)/shard_map/all_gather | solution.py:105
  24.8 0.1 copy.25
  24.8 0.1 reshape.160
  25.0 1.1 fusion.24
  26.1 1.0 fusion.26
  27.1 16.8 %all_gather.15 = bf16[1280,256]{1,0:T(8,128)(2,1)S(1)} all-gather(bf16[320,256]{1,0:T(8,128)(2,1)S(1)} %fusion.26), channel_id=1, replica_groups=mesh['grp'=2,'sp'=4,'tp'=4] {'sp'}, dimensions={0}, use_global_device_ids=true | all-gather | bytes 819200 | tf_op jit(solution)/shard_map/all_gather | solution.py:104
  43.9 0.2 copy.24
  44.2 1.0 constant_dynamic-slice_fusion
  45.2 15.2 %while.15 = (s32[]{:T(128)}, f32[4,320]{1,0:T(4,128)S(1)}, f32[4,320]{1,0:T(4,128)S(1)}, f32[320,4,64]{0,2,1:T(8,128)S(1)}, bf16[2,640,256]{2,1,0:T(8,128)(2,1)S...) while((s32[]{:T(128)}, f32[4,320]{1,0:T(4,128)S(1)}, ...), condition=%wide.region_4.5_spmd.clone, body=%wide.region_1.4_spmd.clone.sunk | while | flops 436231680 | bytes 32759976 | solution.py:119
  45.2 0.3 convolution_convert_fusion.6
  45.5 0.6 fusion.74
  46.1 2.4 fusion.75
  48.5 0.3 convolution_convert_fusion.7
  48.8 2.9 fusion.79
  51.8 1.0 fusion.77
  52.8 0.3 convolution_convert_fusion.6
  53.1 0.6 fusion.74
  53.7 2.4 fusion.75
  56.1 0.3 convolution_convert_fusion.7
  56.4 2.9 fusion.79
  59.3 1.0 fusion.77
  60.4 1.6 convolution_convert_fusion.3
  62.0 0.0 all-reduce.2.cloned.1.call-update
  62.1 0.0 all-gather.5.cloned.1.call-start
  62.1 0.5 all-gather.5.cloned.1.call-update
  62.6 0.0 all-gather.7.cloned.1.call-start
  62.7 0.5 all-gather.7.cloned.1.call-update
  63.2 0.0 all-gather.9.cloned.1.call-start
  63.3 0.5 all-gather.9.cloned.1.call-update
  63.8 0.0 copy-start.4
  63.8 0.0 reduce-scatter.2.cloned.1.call-start
  63.9 37.3 %all-reduce.2.cloned.1.call-done = bf16[320,2048]{1,0:T(8,128)(2,1)} async-done(((bf16[320,2048]{1,0:T(8,128)(2,1)}), bf16[320,2048]{1,0:T(8,128)(2,1)}) %all-reduce.2.cloned.1.call-update) | async-done | bytes 1310736 | tf_op jit(solution)/shard_map/psum | solution.py:129
  101.1 0.0 copy-done.2
  101.1 3.2 convert_add_fusion
  104.4 66.1 %all-gather.5.cloned.1.call-done = bf16[2048,1408]{1,0:T(8,128)(2,1)} async-done(((bf16[512,1408]{1,0:T(8,128)(2,1)}), bf16[2048,1408]{1,0:T(8,128)(2,1)}) %all-gather.5.cloned.1.call-update) | async-done | bytes 5767184 | tf_op jit(solution)/shard_map/all_gather | solution.py:133
  170.5 6.5 %fusion.36 = f32[320,1408]{1,0:T(8,128)} fusion(bf16[2048,1408]{1,0:T(8,128)(2,1)} %all-gather.5.cloned.1.call-done, f32[2048]{0:T(1024)S(1)} %copy-done.4, f32[320]{0:T(512)S(1)} %add_rsqrt_fusion, bf16[320,2048]{1,0:T(8,128)(2,1)} %all-reduce.2.cloned.1.call-done, bf16[320,2048]{1,0:T(8,128)(2,1)S(1)} %copy-done.2), kind=kOutput, calls=%fused_computation.69 | convolution fusion | flops 1849425920 | bytes 10200320 | tf_op jit(solution)/shard_map/dot_general | solution.py:135
  177.0 99.7 %all-gather.7.cloned.1.call-done = bf16[2048,1408]{1,0:T(8,128)(2,1)} async-done(((bf16[512,1408]{1,0:T(8,128)(2,1)}), bf16[2048,1408]{1,0:T(8,128)(2,1)}) %all-gather.7.cloned.1.call-update) | async-done | bytes 5767184 | tf_op jit(solution)/shard_map/all_gather | solution.py:134
  276.8 106.3 %all-gather.9.cloned.1.call-done = bf16[1408,2048]{1,0:T(8,128)(2,1)} async-done(((bf16[1408,512]{1,0:T(8,128)(2,1)}), bf16[1408,2048]{1,0:T(8,128)(2,1)}) %all-gather.9.cloned.1.call-update) | async-done | bytes 5767184 | tf_op jit(solution)/shard_map/all_gather | solution.py:140
  383.0 10.7 %convolution_convert_fusion.2 = bf16[320,2048]{1,0:T(8,128)(2,1)} fusion(bf16[1408,2048]{1,0:T(8,128)(2,1)} %all-gather.9.cloned.1.call-done, bf16[2048,1408]{1,0:T(8,128)(2,1)} %all-gather.7.cloned.1.call-done, f32[320,1408]{1,0:T(8,128)} %fusion.36, f32[2048]{0:T(1024)S(1)} %copy-done.4, f32[320]{0:T(512)S(1)} %add_rsqrt_fusion, ...), kind=kOutput, calls=%fused_computation.27 | convolution fusion | flops 3698278400 | bytes 17278208 | tf_op jit(solution)/shard_map/dot_general | solution.py:138
  393.7 0.0 reduce-scatter.2.cloned.1.call-update
  393.7 24.8 %reduce-scatter.2.cloned.1.call-done = bf16[80,2048]{1,0:T(8,128)(2,1)} async-done(((bf16[320,2048]{1,0:T(8,128)(2,1)}), bf16[80,2048]{1,0:T(8,128)(2,1)}) %reduce-scatter.2.cloned.1.call-update) | async-done | bytes 327696 | tf_op jit(solution)/shard_map/reduce_scatter | solution.py:143
  418.6 2.0 add_convert_fusion
  (29 shorter events, 0.3 us)
Async XLA Ops:
  7.4 53.0 %copy-start = (bf16[256,2048]{1,0:T(8,128)(2,1)S(1)}, bf16[256,2048]{1,0:T(8,128)(2,1)}, u32[]{:S(2)}) copy-start(bf16[256,2048]{1,0:T(8,128)(2,1)} %param.23) | copy-start | bytes 3145732
  7.4 36.6 %copy-start.3 = (bf16[320,256]{1,0:T(8,128)(2,1)S(1)}, bf16[320,256]{1,0:T(8,128)(2,1)}, u32[]{:S(2)}) copy-start(bf16[320,256]{1,0:T(8,128)(2,1)} %param.15) | copy-start | bytes 491524
  7.4 93.8 %all-reduce.2.cloned.1.call-start = ((), (), s32[]{:S(2)}) async-start(), calls=%async_computation.1 | async-start | bytes 2621440 | tf_op jit(solution)/shard_map/psum | solution.py:129
  48.5 3.2 copy-start.1
  56.1 3.2 copy-start.1
  62.0 39.1 %copy-start.2 = (bf16[320,2048]{1,0:T(8,128)(2,1)S(1)}, bf16[320,2048]{1,0:T(8,128)(2,1)}, u32[]{:S(2)}) copy-start(bf16[320,2048]{1,0:T(8,128)(2,1)} %param.22) | copy-start | bytes 3932164
  62.1 108.4 %all-gather.5.cloned.1.call-start = ((), (), s32[]{:S(2)}) async-start(), calls=%async_computation.2 | async-start | bytes 7208960 | tf_op jit(solution)/shard_map/all_gather | solution.py:133
  62.6 214.1 %all-gather.7.cloned.1.call-start = ((), (), s32[]{:S(2)}) async-start(), calls=%async_computation.3 | async-start | bytes 7208960 | tf_op jit(solution)/shard_map/all_gather | solution.py:134
  63.2 319.8 %all-gather.9.cloned.1.call-start = ((), (), s32[]{:S(2)}) async-start(), calls=%async_computation.4 | async-start | bytes 7208960 | tf_op jit(solution)/shard_map/all_gather | solution.py:140
  63.8 106.7 %copy-start.4 = (f32[2048]{0:T(1024)S(1)}, f32[2048]{0:T(1024)}, u32[]{:S(2)}) copy-start(f32[2048]{0:T(1024)} %param.24) | copy-start | bytes 24580
  63.8 354.8 %reduce-scatter.2.cloned.1.call-start = ((), (), s32[]{:S(2)}) async-start(), calls=%async_computation.5 | async-start | bytes 1638400 | tf_op jit(solution)/shard_map/reduce_scatter | solution.py:143
Sparse Core Ops, SparseCore 0:
  62.2 38.9 all-reduce.1
  393.8 24.6 reduce-scatter.1
Sparse Core Ops, SparseCore 1:
  64.1 106.3 all-gather.4
  171.9 104.8 all-gather.6
  278.2 104.8 all-gather.8
where the time goes:
time: 428 us
  waiting for transfers between devices  336 us (79%)
  blocking collectives  31.9 us (7%)
  matrix products  31.9 us (7%)
  between operations  15.2 us (4%)
  other arithmetic  10.5 us (2%)
    all_gather x1, waiting for transfers between devices, local(): lax.all_gather(down_weight, 'sp', axis=1, tiled=True)  106 us
    all_gather x1, waiting for transfers between devices, local(): up_piece = lax.all_gather(up_weight, 'sp', axis=0, tiled=True)  99.7 us
    all_gather x1, waiting for transfers between devices, local(): gate_piece = lax.all_gather(gate_weight, 'sp', axis=0, tiled=True)  66.1 us
    psum x1, waiting for transfers between devices, local(): summed = lax.psum(projected, 'tp').astype(jnp.float32)  37.3 us
    reduce_scatter x1, waiting for transfers between devices, local(): lax.psum_scatter(terms.astype(jnp.bfloat16), 'tp', scatter_dimension=0, t...  24.8 us
    all_gather x1, blocking collectives, local(): latent_piece = lax.all_gather(latent, 'sp', axis=0, tiled=True)  16.8 us
    all_gather x1, blocking collectives, local(): rope_piece = lax.all_gather(key_turned, 'sp', axis=0, tiled=True)  15.1 us
    dot_general x1, matrix products, local(): jnp.dot(hidden, lax.all_gather(down_weight, 'sp', axis=1, tiled=True), pr...  10.7 us
  transfers between devices with their start and end apart: 5, of which 5 were waited for; matrix products, arithmetic and copies ran while one was open for 2% of the time, Pallas kernels for 0%

commit v1 on v0

--- a/solution.py
+++ b/solution.py
@@ -126,7 +126,11 @@
     projected = jnp.dot(attended, out_weight, preferred_element_type=jnp.float32).astype(
         jnp.bfloat16
     )
-    summed = lax.psum(projected, "tp").astype(jnp.float32)
+
+    def perform_wires_for(inputs):
+        return jnp.sum(lax.all_gather(inputs, "tp"), 0)
+
+    summed = perform_wires_for(projected).astype(jnp.float32)
     mixed_all = residual.astype(jnp.float32) + summed
     normed_all = norm_rows(mixed_all, ffn_gain).astype(jnp.bfloat16)
     mixed_own = lax.dynamic_slice_in_dim(mixed_all, tp_index * own_rows, own_rows, 0)

time: 428 us -> 468 us (1.093)
  waiting for transfers between devices: 336 us -> 370 us
  other arithmetic: 10.5 us -> 15.9 us
    all_gather x0 -> x1, waiting for transfers between devices: none -> 38.1 us  [perform_wires_for(): return jnp.sum(lax.all_gather(inputs, 'tp'), 0)]
    psum x1 -> x0, waiting for transfers between devices: 37.3 us -> none  [local(): summed = lax.psum(projected, 'tp').astype(jnp.float32)]
    all_gather x1, waiting for transfers between devices: 66.1 us -> 99.7 us  [local(): gate_piece = lax.all_gather(gate_weight, 'sp', axis=0, tiled=True)]
    all_gather x1, waiting for transfers between devices: 99.7 us -> 106 us  [local(): up_piece = lax.all_gather(up_weight, 'sp', axis=0, tiled=True)]
    all_gather x1, waiting for transfers between devices: 106 us -> 99.6 us  [local(): lax.all_gather(down_weight, 'sp', axis=1, tiled=True)]
    reduce_sum x0 -> x1, other arithmetic: none -> 4.96 us  [perform_wires_for(): return jnp.sum(lax.all_gather(inputs, 'tp'), 0)]
  transfers between devices with their start and end apart: 5 -> 5, of which waited for: 5 -> 5; matrix products, arithmetic and copies ran while one was open for 2% -> 3% of each run, Pallas kernels for 0% -> 0%
where the time goes in v1:
time: 468 us; the launch traced here: 467 us
  waiting for transfers between devices  370 us (79%)
  matrix products  32.6 us (7%)
  blocking collectives  31.9 us (7%)
  other arithmetic  15.9 us (3%)
  between operations  13.3 us (3%)
    all_gather x1, waiting for transfers between devices, local(): up_piece = lax.all_gather(up_weight, 'sp', axis=0, tiled=True)  106 us
    all_gather x1, waiting for transfers between devices, local(): gate_piece = lax.all_gather(gate_weight, 'sp', axis=0, tiled=True)  99.7 us
    all_gather x1, waiting for transfers between devices, local(): lax.all_gather(down_weight, 'sp', axis=1, tiled=True)  99.6 us
    all_gather x1, waiting for transfers between devices, perform_wires_for(): return jnp.sum(lax.all_gather(inputs, 'tp'), 0)  38.1 us
    reduce_scatter x1, waiting for transfers between devices, local(): lax.psum_scatter(terms.astype(jnp.bfloat16), 'tp', scatter_dimension=0, t...  24.8 us
    all_gather x1, blocking collectives, local(): latent_piece = lax.all_gather(latent, 'sp', axis=0, tiled=True)  16.8 us
    all_gather x1, blocking collectives, local(): rope_piece = lax.all_gather(key_turned, 'sp', axis=0, tiled=True)  15.1 us
    dot_general x1, matrix products, local(): jnp.dot(hidden, lax.all_gather(down_weight, 'sp', axis=1, tiled=True), pr...  11 us
  transfers between devices with their start and end apart: 5, of which 5 were waited for; matrix products, arithmetic and copies ran while one was open for 3% of the time, Pallas kernels for 0%

profile of v1, /device:TPU:0, one launch (start us, length us, event | category | flops | bytes accessed | tf_op | source)
XLA Modules:
  0.0 467.2 jit_solution(11834628920532769985)
XLA Ops:
  6.5 0.0 copy-start
  6.6 1.1 copy.26
  7.7 0.7 convert.19
  8.5 0.2 multiply_cosine_fusion
  8.7 0.2 fusion.32
  8.9 15.1 %all-gather.1 = bf16[4,320,32]{1,2,0:T(8,128)(2,1)S(1)} all-gather(bf16[1,320,32]{1,2,0:T(8,128)(2,1)S(1)} %bitcast.84), channel_id=1, replica_groups=mesh['grp'=2,'sp'=4,'tp'=4] {'sp'}, dimensions={0}, use_global_device_ids=true | all-gather | bytes 102400 | tf_op jit(solution)/shard_map/all_gather | solution.py:105
  23.9 0.1 copy.25
  24.0 0.1 reshape.160
  24.2 1.1 fusion.24
  25.2 1.0 fusion.26
  26.3 16.8 %all_gather.21 = bf16[1280,256]{1,0:T(8,128)(2,1)S(1)} all-gather(bf16[320,256]{1,0:T(8,128)(2,1)S(1)} %fusion.26), channel_id=1, replica_groups=mesh['grp'=2,'sp'=4,'tp'=4] {'sp'}, dimensions={0}, use_global_device_ids=true | all-gather | bytes 819200 | tf_op jit(solution)/shard_map/all_gather | solution.py:104
  43.1 0.0 copy-done.2
  43.1 0.2 copy.24
  43.3 1.0 constant_dynamic-slice_fusion
  44.3 15.2 %while.15 = (s32[]{:T(128)}, f32[4,320]{1,0:T(4,128)S(1)}, f32[4,320]{1,0:T(4,128)S(1)}, f32[320,4,64]{0,2,1:T(8,128)S(1)}, bf16[2,640,256]{2,1,0:T(8,128)(2,1)S...) while((s32[]{:T(128)}, f32[4,320]{1,0:T(4,128)S(1)}, ...), condition=%wide.region_4.5_spmd.clone, body=%wide.region_1.4_spmd.clone.sunk | while | flops 436231680 | bytes 32759976 | solution.py:119
  44.3 0.3 convolution_convert_fusion.6
  44.7 0.6 fusion.74
  45.3 2.4 fusion.75
  47.7 0.3 convolution_convert_fusion.7
  48.0 2.9 fusion.79
  50.9 1.0 fusion.77
  51.9 0.3 convolution_convert_fusion.6
  52.3 0.6 fusion.74
  52.9 2.4 fusion.75
  55.3 0.3 convolution_convert_fusion.7
  55.6 2.9 fusion.79
  58.5 1.0 fusion.77
  59.6 1.6 convolution_convert_fusion.3
  61.2 0.0 all-gather.13.cloned.1.call-update
  61.2 0.0 all-gather.7.cloned.1.call-start
  61.3 0.7 all-gather.7.cloned.1.call-update
  62.0 0.0 all-gather.11.cloned.1.call-start
  62.0 0.7 all-gather.11.cloned.1.call-update
  62.7 0.0 all-gather.9.cloned.1.call-start
  62.8 0.5 all-gather.9.cloned.1.call-update
  63.3 0.2 reduce-scatter.2.cloned.1.call-start
  63.5 38.1 %all-gather.13.cloned.1.call-done = bf16[1280,2048]{1,0:T(8,128)(2,1)} async-done(((bf16[320,2048]{1,0:T(8,128)(2,1)}), bf16[1280,2048]{1,0:T(8,128)(2,1)}) %all-gather.13.cloned.1.call-update) | async-done | bytes 5242896 | tf_op jit(solution)/shard_map/all_gather | solution.py:131
  101.6 5.0 %reduce_sum.40 = bf16[320,2048]{1,0:T(8,128)(2,1)} reduce(bf16[4,320,2048]{2,1,0:T(8,128)(2,1)} %bitcast.79, bf16[]{:T(256)} %constant.85.clone.1), dimensions={0}, to_apply=%region_5.6 | reduce | flops 1966080 | bytes 6553602 | tf_op jit(solution)/shard_map/reduce_sum | solution.py:131
  106.6 3.6 convert_add_fusion
  110.2 99.7 %all-gather.7.cloned.1.call-done = bf16[2048,1408]{1,0:T(8,128)(2,1)} async-done(((bf16[512,1408]{1,0:T(8,128)(2,1)}), bf16[2048,1408]{1,0:T(8,128)(2,1)}) %all-gather.7.cloned.1.call-update) | async-done | bytes 5767184 | tf_op jit(solution)/shard_map/all_gather | solution.py:137
  209.9 0.0 copy-done.3
  209.9 6.9 %fusion.36 = f32[320,1408]{1,0:T(8,128)} fusion(bf16[2048,1408]{1,0:T(8,128)(2,1)} %all-gather.7.cloned.1.call-done, f32[2048]{0:T(1024)S(1)} %copy-done.3, f32[320]{0:T(512)S(1)} %add_rsqrt_fusion, bf16[320,2048]{1,0:T(8,128)(2,1)} %reduce_sum.40, bf16[320,2048]{1,0:T(8,128)(2,1)} %param.22), kind=kOutput, calls=%fused_computation.69 | convolution fusion | flops 1849425920 | bytes 10200320 | tf_op jit(solution)/shard_map/dot_general | solution.py:139
  216.8 99.6 %all-gather.11.cloned.1.call-done = bf16[1408,2048]{1,0:T(8,128)(2,1)} async-done(((bf16[1408,512]{1,0:T(8,128)(2,1)}), bf16[1408,2048]{1,0:T(8,128)(2,1)}) %all-gather.11.cloned.1.call-update) | async-done | bytes 5767184 | tf_op jit(solution)/shard_map/all_gather | solution.py:144
  316.4 106.4 %all-gather.9.cloned.1.call-done = bf16[2048,1408]{1,0:T(8,128)(2,1)} async-done(((bf16[512,1408]{1,0:T(8,128)(2,1)}), bf16[2048,1408]{1,0:T(8,128)(2,1)}) %all-gather.9.cloned.1.call-update) | async-done | bytes 5767184 | tf_op jit(solution)/shard_map/all_gather | solution.py:138
  422.8 11.0 %convolution_convert_fusion.2 = bf16[320,2048]{1,0:T(8,128)(2,1)} fusion(bf16[1408,2048]{1,0:T(8,128)(2,1)} %all-gather.11.cloned.1.call-done, bf16[2048,1408]{1,0:T(8,128)(2,1)} %all-gather.9.cloned.1.call-done, f32[320,1408]{1,0:T(8,128)} %fusion.36, f32[2048]{0:T(1024)S(1)} %copy-done.3, f32[320]{0:T(512)S(1)} %add_rsqrt_fusion, ...), kind=kOutput, calls=%fused_computation.27 | convolution fusion | flops 3698278400 | bytes 17278208 | tf_op jit(solution)/shard_map/dot_general | solution.py:142
  433.9 0.0 reduce-scatter.2.cloned.1.call-update
  433.9 24.8 %reduce-scatter.2.cloned.1.call-done = bf16[80,2048]{1,0:T(8,128)(2,1)} async-done(((bf16[320,2048]{1,0:T(8,128)(2,1)}), bf16[80,2048]{1,0:T(8,128)(2,1)}) %reduce-scatter.2.cloned.1.call-update) | async-done | bytes 327696 | tf_op jit(solution)/shard_map/reduce_scatter | solution.py:147
  458.7 2.0 add_convert_fusion
  (28 shorter events, 0.3 us)
Async XLA Ops:
  6.5 53.0 %copy-start = (bf16[256,2048]{1,0:T(8,128)(2,1)S(1)}, bf16[256,2048]{1,0:T(8,128)(2,1)}, u32[]{:S(2)}) copy-start(bf16[256,2048]{1,0:T(8,128)(2,1)} %param.23) | copy-start | bytes 3145732
  6.5 36.6 %copy-start.2 = (bf16[320,256]{1,0:T(8,128)(2,1)S(1)}, bf16[320,256]{1,0:T(8,128)(2,1)}, u32[]{:S(2)}) copy-start(bf16[320,256]{1,0:T(8,128)(2,1)} %param.15) | copy-start | bytes 491524
  6.5 95.0 %all-gather.13.cloned.1.call-start = ((), (), s32[]{:S(2)}) async-start(), calls=%async_computation.5 | async-start | bytes 6553600 | tf_op jit(solution)/shard_map/all_gather | solution.py:131
  47.7 3.3 copy-start.1
  55.3 3.3 copy-start.1
  61.2 148.7 %all-gather.7.cloned.1.call-start = ((), (), s32[]{:S(2)}) async-start(), calls=%async_computation.1 | async-start | bytes 7208960 | tf_op jit(solution)/shard_map/all_gather | solution.py:137
  62.0 254.5 %all-gather.11.cloned.1.call-start = ((), (), s32[]{:S(2)}) async-start(), calls=%async_computation.3 | async-start | bytes 7208960 | tf_op jit(solution)/shard_map/all_gather | solution.py:144
  62.7 360.1 %all-gather.9.cloned.1.call-start = ((), (), s32[]{:S(2)}) async-start(), calls=%async_computation.2 | async-start | bytes 7208960 | tf_op jit(solution)/shard_map/all_gather | solution.py:138
  63.3 395.4 %reduce-scatter.2.cloned.1.call-start = ((), (), s32[]{:S(2)}) async-start(), calls=%async_computation.4 | async-start | bytes 1638400 | tf_op jit(solution)/shard_map/reduce_scatter | solution.py:147
  106.5 103.3 %copy-start.3 = (f32[2048]{0:T(1024)S(1)}, f32[2048]{0:T(1024)}, u32[]{:S(2)}) copy-start(f32[2048]{0:T(1024)} %param.24) | copy-start | bytes 24580
Sparse Core Ops, SparseCore 0:
  61.3 40.1 all-gather.12
  103.2 106.6 all-gather.6
  211.5 104.9 all-gather.10
  317.9 104.9 all-gather.8
  434.0 24.6 reduce-scatter.1
